TPU v7x, 32 devices: a whole 2x2x4 slice. The times are simulated.
32 devices in a mesh: sp: 8 (over z, core), tp: 4 (over y, x).
Axes of the slice: x: 2, y: 2, z: 4, core: 2. Of those that a mesh axis runs over, the one named last changes fastest.
Arguments:
- residual_in: bfloat16 [2048, 2048], P('sp', 'tp'), may hold values from -20 to 20
- conv_value: bfloat16 [2048, 2048], P('sp', 'tp'), may hold values from -6 to 6
- conv_gate: bfloat16 [2048, 2048], P('sp', 'tp'), may hold values from -9 to 9
- doc_ids: int32 [2048], P('sp'), may hold values from 0 to 3, never falling along the last dimension, each value on 1 to 1024 neighbouring positions
- conv_kernel: bfloat16 [31, 2048], P(None, 'tp'), may hold values from -3 to 3
- ln_gain: bfloat16 [2048], P('tp'), may hold values from 0.099609375 to 1.8984375
- out_weight: bfloat16 [2048, 2048], P(None, 'tp'), may hold values from -0.25 to 0.25
- norm_gain: bfloat16 [2048], P('tp'), may hold values from 0.099609375 to 1.8984375
- routes: int32 [2048, 2], P('sp'), may hold values from 0 to 7, all different within a row; in each aligned block of 256 rows (0 to 255, 256 to 511, ...) at most 128 rows name the same one
- route_weight: float32 [2048, 2], P('sp'), may hold values from 0.1 to 1
- gate_w: bfloat16 [8, 2048, 4096], P('sp', None, 'tp'), may hold values from -0.125 to 0.125
- up_w: bfloat16 [8, 2048, 4096], P('sp', None, 'tp'), may hold values from -0.125 to 0.125
- down_w: bfloat16 [8, 4096, 2048], P('sp', 'tp'), may hold values from -0.125 to 0.125
Outputs:
- mixed: bfloat16 [2048, 2048], P('sp', 'tp')
Inputs may be any that keep to these rules, and one draw needn't show every extreme that they name: `routes`: in each aligned block of 256 positions no expert is named by more than 128 positions, a bound that some block reaches; a position's two experts differ. `doc_ids`: never falls along the positions; each document spans 1 to 1024 positions, one exactly that many.
All inputs are finite; a program needn't handle non-finite values.
Results may differ from a plain program's by a relative error of at most 0.012.
Values may be sent and summed in bfloat16 or wider, within the bound.
A program may use at most 64 MiB of HBM per device.

v0:
```python
import functools

import jax
import jax.numpy as jnp
from jax import lax
from jax.experimental import pallas as pl
from jax.experimental.pallas import tpu as pltpu
from jax.sharding import PartitionSpec as P

epsilon = 1e-06
groups = 4


def transposed_dot(a, b):
    return lax.dot_general(a, b, (((0,), (0,)), ((), ())), preferred_element_type=jnp.float32)


def remote(src, dst, send_sem, recv_sem, sp, tp):
    return pltpu.make_async_remote_copy(
        src_ref=src,
        dst_ref=dst,
        send_sem=send_sem,
        recv_sem=recv_sem,
        device_id=(sp, tp),
        device_id_type=pl.DeviceIdType.MESH,
    )


def layer_kernel(
    n_sp,
    n_tp,
    cap,
    residual,
    conv_value,
    conv_gate,
    docs,
    conv_kernel,
    ln_gain,
    norm_gain,
    routes,
    route_weight,
    proj_hbm,
    gate_hbm,
    up_hbm,
    down_hbm,
    mixed,
    proj,
    gate,
    up,
    down,
    taps,
    extended,
    doc_extended,
    since,
    conv,
    tail,
    tail_docs,
    halo,
    halo_docs,
    stats,
    activated,
    projected,
    stream,
    normed,
    chosen,
    outbound,
    slots,
    hidden,
    partial,
    arrived,
    summed,
    returned,
    weight_hi,
    weight_lo,
    local_sem,
    halo_send,
    halo_recv,
    stat_send,
    stat_recv,
    act_send,
    act_recv,
    out_send,
    out_recv,
    spread_send,
    spread_recv,
    sum_send,
    sum_recv,
    back_send,
    back_recv,
):
    sp = lax.axis_index("sp")
    tp = lax.axis_index("tp")
    rows, cols = residual.shape
    width = cols * n_tp
    lookback = conv_kernel.shape[0] - 1
    pad = tail.shape[0]
    per_group = n_sp // groups
    group_rows = per_group * cap
    my_group = sp // per_group
    my_member = sp % per_group
    relays = n_tp == 4
    across_x = tp + 1 - 2 * (tp % 2)
    across_y = (tp + 2) % n_tp
    diagonal = (across_x + 2) % n_tp
    loads = [
        pltpu.make_async_copy(src, dst, local_sem.at[i])
        for i, (src, dst) in enumerate(
            ((proj_hbm, proj), (gate_hbm, gate), (up_hbm, up), (down_hbm, down))
        )
    ]
    for load in loads:
        load.start()

    barrier = pltpu.get_barrier_semaphore()
    for i in range(1, n_sp):
        pl.semaphore_signal(
            barrier, inc=1, device_id=((sp + i) % n_sp, tp), device_id_type=pl.DeviceIdType.MESH
        )
    for i in range(1, n_tp):
        pl.semaphore_signal(
            barrier, inc=1, device_id=(sp, (tp + i) % n_tp), device_id_type=pl.DeviceIdType.MESH
        )
    sends = []

    def go(*args):
        send = remote(*args)
        send.start()
        sends.append(send)

    def landed(ref, sem):
        remote(ref, ref, act_send.at[0], sem, sp, tp).wait_recv()

    def col_block(t):
        return pl.ds(pl.multiple_of(t * cols, 128), cols)

    def spread_start(ref, start, size, ss, rs):
        block = ref.at[pl.ds(start, size), col_block(tp)]
        if relays:
            go(block, block, ss(1), rs(1), sp, across_x)
            go(block, block, ss(2), rs(2), sp, across_y)
        else:
            for j in range(1, n_tp):
                go(block, block, ss(j), rs(j), sp, (tp + j) % n_tp)

    def spread_relay(ref, start, size, ss, rs):
        if relays:
            half = size // 2
            landed(ref.at[pl.ds(start, size), col_block(across_x)], rs(1))
            block = ref.at[pl.ds(start, half), col_block(across_x)]
            go(block, block, ss(3), rs(3), sp, across_y)
            landed(ref.at[pl.ds(start, size), col_block(across_y)], rs(2))
            block = ref.at[pl.ds(start + half, half), col_block(across_y)]
            go(block, block, ss(0), rs(0), sp, across_x)

    def spread_finish(ref, start, size, rs):
        if relays:
            half = size // 2
            landed(ref.at[pl.ds(start, half), col_block(diagonal)], rs(3))
            landed(ref.at[pl.ds(start + half, half), col_block(diagonal)], rs(0))
        else:
            for j in range(1, n_tp):
                landed(
                    ref.at[pl.ds(start, size), col_block((tp - j + n_tp) % n_tp)], rs(j)
                )

    def stats_start(i, first, second):
        lane = lax.broadcasted_iota(jnp.int32, (rows, 128), 1)
        both = jnp.where(lane == 0, first, jnp.where(lane == 1, second, 0.0))
        stats[i, 0] = jnp.transpose(both)[0:8]
        for j in range(1, n_tp):
            go(
                stats.at[i, 0],
                stats.at[i, j],
                stat_send.at[i, j],
                stat_recv.at[i, j],
                sp,
                (tp + j) % n_tp,
            )

    def stats_finish(i):
        total = stats[i, 0]
        for j in range(1, n_tp):
            landed(stats.at[i, j], stat_recv.at[i, j])
            total = total + stats[i, j]
        back = jnp.transpose(jnp.concatenate([total] * 16, 0))
        return back[:, 0:1], back[:, 1:2]

    gated = (
        conv_value[...].astype(jnp.float32) * jax.nn.sigmoid(conv_gate[...].astype(jnp.float32))
    ).astype(jnp.bfloat16)
    extended[pl.ds(pad, rows), :] = gated.astype(jnp.float32)
    tail[...] = gated[rows - pad :]
    doc_rows = jnp.transpose(
        jnp.broadcast_to(docs[...].astype(jnp.float32), (128, rows))
    )
    doc_extended[pl.ds(pad, rows), :] = doc_rows
    tail_docs[...] = doc_rows[rows - pad :]
    taps[...] = conv_kernel[...].astype(jnp.float32)
    pl.semaphore_wait(barrier, n_sp - 1 + n_tp - 1)
    next_sp = (sp + 1) % n_sp
    tails = [
        remote(tail, halo, halo_send.at[0], halo_recv.at[0], next_sp, tp),
        remote(tail_docs, halo_docs, halo_send.at[1], halo_recv.at[1], next_sp, tp),
    ]
    for send in tails:
        send.start()
        sends.append(send)

    part = min(64, rows)

    def convolve(r):
        here = pl.ds(r * part, part)
        own = doc_extended[pl.ds(pad + r * part, part), :]
        count = jnp.zeros((part, 128), jnp.float32)
        for back in range(1, lookback + 1):
            count = count + jnp.where(
                doc_extended[pl.ds(pad + r * part - back, part), :] == own, 1.0, 0.0
            )
        since[here, :] = count

        @pl.loop(0, cols // 128)
        def _(c):
            at = pl.ds(pl.multiple_of(c * 128, 128), 128)
            reach = since[here, :]
            total = jnp.zeros((part, 128), jnp.float32)
            for tap in range(lookback + 1):
                value = extended[pl.ds(pad - lookback + r * part + tap, part), at]
                total = total + jnp.where(
                    reach >= lookback - tap, value * taps[tap : tap + 1, at], 0.0
                )
            conv[here, at] = total

    for r in range(1, rows // part):
        convolve(r)
    landed(halo, halo_recv.at[0])
    landed(halo_docs, halo_recv.at[1])
    inside = sp > 0
    extended[pl.ds(0, pad), :] = jnp.where(inside, halo[...].astype(jnp.float32), 0.0)
    doc_extended[pl.ds(0, pad), :] = jnp.where(inside, halo_docs[...], -1.0)
    convolve(0)
    conv_out = conv[...]
    stats_start(
        0,
        jnp.sum(conv_out, 1, keepdims=True),
        jnp.sum(conv_out * conv_out, 1, keepdims=True),
    )

    expert_id = lax.broadcasted_iota(jnp.int32, (rows, n_sp), 1)
    first = routes[:, 0:1] == expert_id
    second = routes[:, 1:2] == expert_id
    named = jnp.where(first | second, 1.0, 0.0)
    earlier = jnp.where(
        lax.broadcasted_iota(jnp.int32, (rows, rows), 1)
        < lax.broadcasted_iota(jnp.int32, (rows, rows), 0),
        1.0,
        0.0,
    ).astype(jnp.bfloat16)
    rank = jnp.dot(earlier, named.astype(jnp.bfloat16), preferred_element_type=jnp.float32)
    slot = jnp.where(first | second, rank, -1.0).astype(jnp.int32)
    weight = jnp.where(first, route_weight[:, 0:1], 0.0) + jnp.where(
        second, route_weight[:, 1:2], 0.0
    )
    slot_id = lax.broadcasted_iota(jnp.int32, (rows, cap), 1)
    for e in range(n_sp):
        chosen[e] = jnp.where(slot[:, e : e + 1] == slot_id, 1.0, 0.0).astype(jnp.bfloat16)

    channel_sum, channel_sq = stats_finish(0)
    mean = channel_sum / width
    scale = lax.rsqrt(channel_sq / width - mean * mean + epsilon)
    v = (conv[...] - mean) * scale * ln_gain[...].astype(jnp.float32)
    activated[:, col_block(tp)] = (v * jax.nn.sigmoid(v)).astype(jnp.bfloat16)

    def act_block(i):
        return act_send.at[i]

    def act_arrival(i):
        return act_recv.at[i]

    spread_start(activated, 0, rows, act_block, act_arrival)
    loads[0].wait()

    def project(t):
        return jnp.dot(
            activated[:, col_block(t)],
            proj[pl.ds(pl.multiple_of(t * cols, 128), cols), :],
            preferred_element_type=jnp.float32,
        )

    projected[...] = project(tp)
    for e in range(n_sp):
        at = jnp.where(slot[:, e : e + 1] == slot_id, weight[:, e : e + 1], 0.0)
        hi = at.astype(jnp.bfloat16)
        weight_hi[e] = hi
        weight_lo[e] = (at - hi.astype(jnp.float32)).astype(jnp.bfloat16)
    spread_relay(activated, 0, rows, act_block, act_arrival)
    if relays:
        projected[...] += project(across_x) + project(across_y)
    spread_finish(activated, 0, rows, act_arrival)
    if relays:
        projected[...] += project(diagonal)
    else:
        for j in range(1, n_tp):
            projected[...] += project((tp + j) % n_tp)
    stream[...] = (
        residual[...].astype(jnp.float32)
        + projected[...].astype(jnp.bfloat16).astype(jnp.float32)
    ).astype(jnp.bfloat16)
    stream_part = stream[...].astype(jnp.float32)
    square = jnp.sum(stream_part * stream_part, 1, keepdims=True)
    stats_start(1, square, square)
    row_total, _ = stats_finish(1)
    normed[...] = (
        stream[...].astype(jnp.float32)
        * lax.rsqrt(row_total / width + epsilon)
        * norm_gain[...].astype(jnp.float32)
    ).astype(jnp.bfloat16)

    def source_rows(s):
        return pl.ds(pl.multiple_of(s * cap, cap), cap)

    def group_start(k):
        return pl.multiple_of((my_group + k) % groups * group_rows, group_rows)

    for k in range(groups):
        for j in range(per_group):
            dest = (my_group - k + groups) % groups * per_group + (my_member + j) % per_group
            rows_out = transposed_dot(chosen[dest], normed[...]).astype(jnp.bfloat16)
            if k == 0 and j == 0:
                slots[source_rows(sp), col_block(tp)] = rows_out
                continue
            outbound[dest] = rows_out
            go(
                outbound.at[dest],
                slots.at[source_rows(sp), col_block(tp)],
                out_send.at[k * per_group + j],
                out_recv.at[sp],
                dest,
                tp,
            )

    def spread_sems(sems, k):
        return lambda i: sems.at[k, i]

    def spread(k):
        for j in range(per_group):
            if k == 0 and j == 0:
                continue
            source = (my_group + k) % groups * per_group + (my_member + j) % per_group
            landed(slots.at[source_rows(source), col_block(tp)], out_recv.at[source])
        spread_start(
            slots, group_start(k), group_rows, spread_sems(spread_send, k), spread_sems(spread_recv, k)
        )

    def relay(k):
        spread_relay(
            slots, group_start(k), group_rows, spread_sems(spread_send, k), spread_sems(spread_recv, k)
        )

    half = group_rows // 2
    low, high = pl.ds(0, half), pl.ds(half, half)

    def compute(k):
        spread_finish(slots, group_start(k), group_rows, spread_sems(spread_recv, k))
        x = pl.ds(group_start(k), group_rows)
        units = gate.shape[1]
        tile = min(256, units)

        @pl.loop(0, units // tile)
        def _(n):
            at = pl.ds(pl.multiple_of(n * tile, tile), tile)
            g = jnp.dot(slots[x, :], gate[:, at], preferred_element_type=jnp.float32)
            u = jnp.dot(slots[x, :], up[:, at], preferred_element_type=jnp.float32)
            hidden[:, at] = (g * jax.nn.sigmoid(g) * u).astype(jnp.bfloat16)

        @pl.loop(0, width // 256)
        def _(n):
            at = pl.ds(pl.multiple_of(n * 256, 256), 256)
            partial[k, :, at] = jnp.dot(
                hidden[...], down[:, at], preferred_element_type=jnp.float32
            ).astype(jnp.bfloat16)

        if relays:
            for i, (part_rows, block, peer) in enumerate(
                (
                    (low, across_x, across_x),
                    (low, diagonal, across_x),
                    (high, across_y, across_y),
                    (high, diagonal, across_y),
                )
            ):
                go(
                    partial.at[k, part_rows, col_block(block)],
                    arrived.at[k, i, low],
                    sum_send.at[k, i],
                    sum_recv.at[k, i],
                    sp,
                    peer,
                )
        else:
            for j in range(1, n_tp):
                peer = (tp + j) % n_tp
                go(
                    partial.at[k, :, col_block(peer)],
                    arrived.at[k, j],
                    sum_send.at[k, j],
                    sum_recv.at[k, j],
                    sp,
                    peer,
                )

    def pass_on(k):
        if relays:
            for i, (part_rows, peer) in enumerate(((low, across_y), (high, across_x))):
                landed(arrived.at[k, 2 * i + 1, low], sum_recv.at[k, 2 * i + 1])
                arrived[k, 2 + i, high] = (
                    partial[k, part_rows, col_block(peer)].astype(jnp.float32)
                    + arrived[k, 2 * i + 1, low].astype(jnp.float32)
                ).astype(jnp.bfloat16)
                go(
                    arrived.at[k, 2 + i, high],
                    arrived.at[k, i, high],
                    sum_send.at[k, 4 + i],
                    sum_recv.at[k, 4 + i],
                    sp,
                    peer,
                )

    def give_back(k):
        if relays:
            for i, part_rows in enumerate((low, high)):
                landed(arrived.at[k, 2 * i, low], sum_recv.at[k, 2 * i])
                landed(arrived.at[k, i, high], sum_recv.at[k, 4 + i])
                summed[k, part_rows] = (
                    partial[k, part_rows, col_block(tp)].astype(jnp.float32)
                    + arrived[k, 2 * i, low].astype(jnp.float32)
                    + arrived[k, i, high].astype(jnp.float32)
                ).astype(jnp.bfloat16)
        else:
            total = partial[k, :, col_block(tp)].astype(jnp.float32)
            for j in range(1, n_tp):
                landed(arrived.at[k, j], sum_recv.at[k, j])
                total = total + arrived[k, j].astype(jnp.float32)
            summed[k] = total.astype(jnp.bfloat16)
        for j in range(per_group):
            member = (my_member + j) % per_group
            source = (my_group + k) % groups * per_group + member
            part = pl.ds(pl.multiple_of(member * cap, cap), cap)
            if k == 0 and j == 0:
                returned[sp] = summed[k, part, :]
                continue
            go(
                summed.at[k, part, :],
                returned.at[sp],
                back_send.at[k * per_group + j],
                back_recv.at[sp],
                source,
                tp,
            )

    spread(0)
    spread(1)
    relay(0)
    spread(2)
    relay(1)
    for load in loads[1:]:
        load.wait()
    compute(0)
    spread(3)
    relay(2)
    compute(1)
    pass_on(0)
    relay(3)
    compute(2)
    pass_on(1)
    give_back(0)
    compute(3)
    pass_on(2)
    give_back(1)
    pass_on(3)
    give_back(2)
    give_back(3)
    for i in range(1, n_sp):
        e = (sp + i) % n_sp
        landed(returned.at[e], back_recv.at[e])
    routed = jnp.zeros((rows, cols), jnp.float32)
    for e in range(n_sp):
        routed = routed + jnp.dot(weight_hi[e], returned[e], preferred_element_type=jnp.float32)
        routed = routed + jnp.dot(weight_lo[e], returned[e], preferred_element_type=jnp.float32)
    mixed[...] = (stream[...].astype(jnp.float32) + routed).astype(jnp.bfloat16)
    for send in sends:
        send.wait_send()


def per_device(
    residual_in,
    conv_value,
    conv_gate,
    doc_ids,
    conv_kernel,
    ln_gain,
    out_weight,
    norm_gain,
    routes,
    route_weight,
    gate_w,
    up_w,
    down_w,
):
    rows, cols = residual_in.shape
    n_sp = lax.axis_size("sp")
    n_tp = lax.axis_size("tp")
    cap = 4 * rows // n_sp
    _, width, units = gate_w.shape
    group_rows = n_sp // groups * cap
    taps = conv_kernel.shape[0]
    pad = (taps - 1 + 15) // 16 * 16
    bf16, f32 = jnp.bfloat16, jnp.float32
    dma = pltpu.SemaphoreType.DMA
    vmem = pl.BlockSpec(memory_space=pltpu.VMEM)
    anywhere = pl.BlockSpec(memory_space=pl.ANY)
    return pl.pallas_call(
        functools.partial(layer_kernel, n_sp, n_tp, cap),
        out_shape=jax.ShapeDtypeStruct((rows, cols), bf16),
        in_specs=[vmem] * 9 + [anywhere] * 4,
        out_specs=vmem,
        scratch_shapes=[
            pltpu.VMEM((width, cols), bf16),
            pltpu.VMEM((width, units), bf16),
            pltpu.VMEM((width, units), bf16),
            pltpu.VMEM((units, width), bf16),
            pltpu.VMEM((taps, cols), f32),
            pltpu.VMEM((pad + rows, cols), f32),
            pltpu.VMEM((pad + rows, 128), f32),
            pltpu.VMEM((rows, 128), f32),
            pltpu.VMEM((rows, cols), f32),
            pltpu.VMEM((pad, cols), bf16),
            pltpu.VMEM((pad, 128), f32),
            pltpu.VMEM((pad, cols), bf16),
            pltpu.VMEM((pad, 128), f32),
            pltpu.VMEM((2, n_tp, 8, rows), f32),
            pltpu.VMEM((rows, width), bf16),
            pltpu.VMEM((rows, cols), f32),
            pltpu.VMEM((rows, cols), bf16),
            pltpu.VMEM((rows, cols), bf16),
            pltpu.VMEM((n_sp, rows, cap), bf16),
            pltpu.VMEM((n_sp, cap, cols), bf16),
            pltpu.VMEM((n_sp * cap, width), bf16),
            pltpu.VMEM((group_rows, units), bf16),
            pltpu.VMEM((groups, group_rows, width), bf16),
            pltpu.VMEM((groups, n_tp, group_rows, cols), bf16),
            pltpu.VMEM((groups, group_rows, cols), bf16),
            pltpu.VMEM((n_sp, cap, cols), bf16),
            pltpu.VMEM((n_sp, rows, cap), bf16),
            pltpu.VMEM((n_sp, rows, cap), bf16),
            dma((4,)),
            dma((2,)),
            dma((2,)),
            dma((2, n_tp)),
            dma((2, n_tp)),
            dma((n_tp,)),
            dma((n_tp,)),
            dma((n_sp,)),
            dma((n_sp,)),
            dma((groups, n_tp)),
            dma((groups, n_tp)),
            dma((groups, n_tp + 2)),
            dma((groups, n_tp + 2)),
            dma((n_sp,)),
            dma((n_sp,)),
        ],
        compiler_params=pltpu.CompilerParams(
            collective_id=0, has_side_effects=True, vmem_limit_bytes=54 << 20
        ),
    )(
        residual_in,
        conv_value,
        conv_gate,
        doc_ids.reshape(1, rows),
        conv_kernel,
        ln_gain.reshape(1, cols),
        norm_gain.reshape(1, cols),
        routes,
        route_weight,
        out_weight,
        gate_w[0],
        up_w[0],
        down_w[0],
    )


def solution(mesh):
    in_specs = (
        P("sp", "tp"),
        P("sp", "tp"),
        P("sp", "tp"),
        P("sp"),
        P(None, "tp"),
        P("tp"),
        P(None, "tp"),
        P("tp"),
        P("sp", None),
        P("sp", None),
        P("sp", None, "tp"),
        P("sp", None, "tp"),
        P("sp", "tp", None),
    )
    out_specs = P("sp", "tp")
    return jax.shard_map(
        per_device, mesh=mesh, in_specs=in_specs, out_specs=out_specs, check_vma=False
    )
```

profile of v0, /device:TPU:25, one launch (start us, length us, event | category | flops | bytes accessed | tf_op | source)
XLA Modules:
  0.0 130.3 jit_solution(4007573367329985842)
XLA Ops:
  0.0 1.3 reshape.10.ln_gain
  1.3 1.2 reshape.11.norm_gain
  2.5 1.5 %copy.14.routes = s32[256,2]{1,0:T(8,128)} copy(s32[256,2]{0,1:T(2,128)} %param.21) | data formatting | bytes 4096 | tf_op args[8]
  4.0 1.5 %copy.15.route_weight = f32[256,2]{1,0:T(8,128)} copy(f32[256,2]{0,1:T(2,128)} %param.22) | data formatting | bytes 4096 | tf_op args[9]
  5.5 123.2 %shard_map.127 = bf16[256,512]{1,0:T(8,128)(2,1)} custom-call(bf16[256,512]{1,0:T(8,128)(2,1)} %residual.1, bf16[256,512]{1,0:T(8,128)(2,1)} %conv_value.1, bf16[256,512]{1,0:T(8,128)(2,1)} %conv_gate.1, s32[1,256]{1,0:T(1,128)} %bitcast.7, bf16[31,512]{1,0:T(8,128)(2,1)} %conv_kernel.1, bf16[1,512]{1,0:T(2,128)(2,1)} %reshape.10.ln_gain, ...), custom_call_target="tpu_custom_call" | custom-call | tf_op jit(solution)/shard_map/pallas_call | solution.py:521
  128.7 1.7 %copy.17 = bf16[256,512]{1,0:T(8,128)(2,1)} copy(bf16[256,512]{1,0:T(8,128)(2,1)} %shard_map.127) | data formatting | bytes 524288
where the time goes:
time: 131 us; the launch traced here: 130 us
  Pallas kernels  123 us (94%)
  local copies, waits for them, and re-layouts  7.12 us (5%)
    pallas_call x1, Pallas kernels, per_device(): pl.pallas_call(functools.partial(layer_kernel, n_sp, n_tp, cap), out_shap...  123 us
    unnamed x3, local copies, waits for them, and re-layouts  4.62 us

commit v1 on v0

--- a/solution.py
+++ b/solution.py
@@ -491,6 +491,614 @@
         send.wait_send()
 
 
+def fused_kernel(
+    n_sp,
+    n_tp,
+    cap,
+    residual,
+    conv_value,
+    conv_gate,
+    docs,
+    conv_kernel,
+    ln_gain,
+    norm_gain,
+    routes,
+    route_weight,
+    proj_hbm,
+    gate_hbm,
+    up_hbm,
+    down_hbm,
+    mixed,
+    proj,
+    gate,
+    up,
+    down,
+    taps,
+    extended,
+    doc_extended,
+    since,
+    conv,
+    tail,
+    tail_docs,
+    halo,
+    halo_docs,
+    stats,
+    plans,
+    scales,
+    activated,
+    projected,
+    stream,
+    tokens,
+    picks,
+    blends,
+    slots,
+    hidden,
+    pairs,
+    outbound,
+    blended,
+    arrived,
+    summed,
+    returned,
+    local_sem,
+    halo_send,
+    halo_recv,
+    stat_send,
+    stat_recv,
+    plan_send,
+    plan_recv,
+    scale_send,
+    scale_recv,
+    act_send,
+    act_recv,
+    plane_send,
+    plane_recv,
+    spread_send,
+    spread_recv,
+    twin_send,
+    twin_recv,
+    swap_send,
+    swap_recv,
+    sum_send,
+    sum_recv,
+    back_send,
+    back_recv,
+):
+    sp = lax.axis_index("sp")
+    tp = lax.axis_index("tp")
+    rows, cols = residual.shape
+    width = cols * n_tp
+    lookback = conv_kernel.shape[0] - 1
+    pad = tail.shape[0]
+    planes = n_sp // 2
+    plane = sp // 2
+    core = sp % 2
+    twin = plane * 2 + 1 - core
+    chunk = rows // 2
+    half = chunk // 2
+    across_x = tp + 1 - 2 * (tp % 2)
+    across_y = (tp + 2) % n_tp
+    diagonal = (across_x + 2) % n_tp
+    loads = [
+        pltpu.make_async_copy(src, dst, local_sem.at[i])
+        for i, (src, dst) in enumerate(
+            ((proj_hbm, proj), (gate_hbm, gate), (up_hbm, up), (down_hbm, down))
+        )
+    ]
+    for load in loads:
+        load.start()
+
+    barrier = pltpu.get_barrier_semaphore()
+    for i in range(1, n_sp):
+        pl.semaphore_signal(
+            barrier, inc=1, device_id=((sp + i) % n_sp, tp), device_id_type=pl.DeviceIdType.MESH
+        )
+    for i in range(1, n_tp):
+        pl.semaphore_signal(
+            barrier, inc=1, device_id=(sp, (tp + i) % n_tp), device_id_type=pl.DeviceIdType.MESH
+        )
+    sends = []
+
+    def go(*args):
+        send = remote(*args)
+        send.start()
+        sends.append(send)
+
+    def landed(ref, sem):
+        remote(ref, ref, act_send.at[0, 0], sem, sp, tp).wait_recv()
+
+    def col_block(t):
+        return pl.ds(pl.multiple_of(t * cols, 128), cols)
+
+    def row_block(start, size):
+        return pl.ds(pl.multiple_of(start, size), size)
+
+    def spread_start(ref, start, ss, rs):
+        block = ref.at[row_block(start, chunk), col_block(tp)]
+        go(block, block, ss(1), rs(1), sp, across_x)
+        go(block, block, ss(2), rs(2), sp, across_y)
+
+    def spread_relay(ref, start, ss, rs):
+        landed(ref.at[row_block(start, chunk), col_block(across_x)], rs(1))
+        block = ref.at[row_block(start, half), col_block(across_x)]
+        go(block, block, ss(3), rs(3), sp, across_y)
+        landed(ref.at[row_block(start, chunk), col_block(across_y)], rs(2))
+        block = ref.at[row_block(start + half, half), col_block(across_y)]
+        go(block, block, ss(0), rs(0), sp, across_x)
+
+    def spread_finish(ref, start, rs):
+        landed(ref.at[row_block(start, half), col_block(diagonal)], rs(3))
+        landed(ref.at[row_block(start + half, half), col_block(diagonal)], rs(0))
+
+    def stats_start(i, q, first, second):
+        lane = lax.broadcasted_iota(jnp.int32, (chunk, 128), 1)
+        both = jnp.where(lane == 0, first, jnp.where(lane == 1, second, 0.0))
+        stats[i, q, 0] = jnp.transpose(both)[0:8]
+        for j in range(1, n_tp):
+            go(
+                stats.at[i, q, 0],
+                stats.at[i, q, j],
+                stat_send.at[i, q, j],
+                stat_recv.at[i, q, j],
+                sp,
+                (tp + j) % n_tp,
+            )
+
+    def stats_total(i, q):
+        total = stats[i, q, 0]
+        for j in range(1, n_tp):
+            landed(stats.at[i, q, j], stat_recv.at[i, q, j])
+            total = total + stats[i, q, j]
+        return total
+
+    def gain_row(ref):
+        return jnp.concatenate(
+            [ref[i : i + 1, :].astype(jnp.float32) for i in range(cols // 128)], 1
+        )
+
+    gated = (
+        conv_value[...].astype(jnp.float32) * jax.nn.sigmoid(conv_gate[...].astype(jnp.float32))
+    ).astype(jnp.bfloat16)
+    extended[pl.ds(pad, rows), :] = gated.astype(jnp.float32)
+    tail[...] = gated[rows - pad :]
+    doc_rows = jnp.transpose(jnp.broadcast_to(docs[...].astype(jnp.float32), (128, rows)))
+    doc_extended[pl.ds(pad, rows), :] = doc_rows
+    tail_docs[...] = doc_rows[rows - pad :]
+    taps[...] = conv_kernel[...].astype(jnp.float32)
+    plans[sp] = jnp.concatenate(
+        [routes[...].astype(jnp.float32), route_weight[...], jnp.zeros((4, rows), jnp.float32)], 0
+    )
+    pl.semaphore_wait(barrier, n_sp - 1 + n_tp - 1)
+    next_sp = (sp + 1) % n_sp
+    go(tail, halo, halo_send.at[0], halo_recv.at[0], next_sp, tp)
+    go(tail_docs, halo_docs, halo_send.at[1], halo_recv.at[1], next_sp, tp)
+    for i in range(1, n_sp):
+        go(plans.at[sp], plans.at[sp], plan_send.at[i], plan_recv.at[sp], (sp + i) % n_sp, tp)
+
+    part = min(64, chunk)
+
+    def convolve(r):
+        here = pl.ds(r * part, part)
+        own = doc_extended[pl.ds(pad + r * part, part), :]
+        count = jnp.zeros((part, 128), jnp.float32)
+        for back in range(1, lookback + 1):
+            count = count + jnp.where(
+                doc_extended[pl.ds(pad + r * part - back, part), :] == own, 1.0, 0.0
+            )
+        since[here, :] = count
+
+        @pl.loop(0, cols // 128)
+        def _(c):
+            at = pl.ds(pl.multiple_of(c * 128, 128), 128)
+            reach = since[here, :]
+            total = jnp.zeros((part, 128), jnp.float32)
+            for tap in range(lookback + 1):
+                value = extended[pl.ds(pad - lookback + r * part + tap, part), at]
+                total = total + jnp.where(
+                    reach >= lookback - tap, value * taps[tap : tap + 1, at], 0.0
+                )
+            conv[here, at] = total
+
+    def channel_stats(q):
+        conv_out = conv[pl.ds(q * chunk, chunk), :]
+        stats_start(
+            0,
+            q,
+            jnp.sum(conv_out, 1, keepdims=True),
+            jnp.sum(conv_out * conv_out, 1, keepdims=True),
+        )
+
+    def sems(ref, *index):
+        return lambda i: ref.at[(*index, i)]
+
+    def activate(q):
+        here = pl.ds(q * chunk, chunk)
+        back = jnp.transpose(jnp.concatenate([stats_total(0, q)] * 16, 0))
+        mean = back[:, 0:1] / width
+        scale = lax.rsqrt(back[:, 1:2] / width - mean * mean + epsilon)
+        v = (conv[here, :] - mean) * scale * gain_row(ln_gain)
+        activated[here, col_block(tp)] = (v * jax.nn.sigmoid(v)).astype(jnp.bfloat16)
+        spread_start(activated, q * chunk, sems(act_send, q), sems(act_recv, q))
+
+    def project(q, t):
+        return jnp.dot(
+            activated[pl.ds(q * chunk, chunk), col_block(t)],
+            proj[col_block(t), :],
+            preferred_element_type=jnp.float32,
+        )
+
+    parts = chunk // part
+    for r in range(parts, 2 * parts):
+        convolve(r)
+    channel_stats(1)
+    for r in range(1, parts):
+        convolve(r)
+    landed(halo, halo_recv.at[0])
+    landed(halo_docs, halo_recv.at[1])
+    inside = sp > 0
+    extended[pl.ds(0, pad), :] = jnp.where(inside, halo[...].astype(jnp.float32), 0.0)
+    doc_extended[pl.ds(0, pad), :] = jnp.where(inside, halo_docs[...], -1.0)
+    convolve(0)
+    channel_stats(0)
+    activate(1)
+    activate(0)
+
+    for i in range(1, n_sp):
+        e = (sp + i) % n_sp
+        landed(plans.at[e], plan_recv.at[e])
+    token = lax.broadcasted_iota(jnp.int32, (rows, rows), 0)
+    later = jnp.where(
+        token < lax.broadcasted_iota(jnp.int32, (rows, rows), 1), 1.0, 0.0
+    ).astype(jnp.bfloat16)
+    slot_id = lax.broadcasted_iota(jnp.int32, (cap, rows), 0)
+
+    def named_by(s, expert):
+        plan = plans[s]
+        first = plan[0:1] == expert
+        second = plan[1:2] == expert
+        weight = jnp.where(first, plan[2:3], 0.0) + jnp.where(second, plan[3:4], 0.0)
+        return jnp.where(first | second, 1.0, 0.0), weight
+
+    def slots_of(sources, expert):
+        both = [named_by(s, expert) for s in sources]
+        named = jnp.concatenate([n for n, _ in both] + [jnp.zeros_like(both[0][0])] * (8 - len(both)), 0)
+        rank = jnp.dot(named.astype(jnp.bfloat16), later, preferred_element_type=jnp.float32)
+        slot = jnp.where(named > 0.5, rank, -1.0).astype(jnp.int32)
+        return [(slot[i : i + 1], weight) for i, (_, weight) in enumerate(both)]
+
+    mine = slots_of([2 * p + core for p in range(planes)], sp.astype(jnp.float32))
+    rest = slots_of([2 * p + 1 - core for p in range(planes)], sp.astype(jnp.float32))
+    other = slots_of([2 * p + core for p in range(planes)], twin.astype(jnp.float32))
+    for p in range(planes):
+        slot, weight = mine[p]
+        picks[p, 0:cap] = jnp.where(slot == slot_id, 1.0, 0.0).astype(jnp.bfloat16)
+        blends[p, 0:cap] = jnp.where(slot == slot_id, weight, 0.0).astype(jnp.bfloat16)
+        slot, weight = rest[p]
+        picks[p, cap : 2 * cap] = jnp.where(slot == slot_id, 1.0, 0.0).astype(jnp.bfloat16)
+        slot, weight = other[p]
+        blends[p, cap : 2 * cap] = jnp.where(slot == slot_id, weight, 0.0).astype(jnp.bfloat16)
+
+    near = [0]
+    for d in range(1, planes // 2 + 1):
+        near += [d] if 2 * d == planes else [d, planes - d]
+
+    def source(k):
+        return (plane + k) % planes * 2 + core
+
+    def first_row(k, q):
+        return source(k) * rows + q * chunk
+
+    def residual_rows(q):
+        here = pl.ds(q * chunk, chunk)
+        spread_relay(activated, q * chunk, sems(act_send, q), sems(act_recv, q))
+        projected[here, :] += project(q, across_x) + project(q, across_y)
+        spread_finish(activated, q * chunk, sems(act_recv, q))
+        total = projected[here, :] + project(q, diagonal)
+        stream_rows = (
+            residual[here, :].astype(jnp.float32)
+            + total.astype(jnp.bfloat16).astype(jnp.float32)
+        ).astype(jnp.bfloat16)
+        stream[here, :] = stream_rows
+        stream_part = stream_rows.astype(jnp.float32)
+        tokens[row_block(first_row(0, q), chunk), col_block(tp)] = (
+            stream_part * gain_row(norm_gain)
+        ).astype(jnp.bfloat16)
+        block = tokens.at[row_block(first_row(0, q), chunk), col_block(tp)]
+        spread_start(tokens, first_row(0, q), sems(spread_send, 0, q), sems(spread_recv, 0, q))
+        for k in near[1:]:
+            go(
+                block,
+                block,
+                plane_send.at[k, q],
+                plane_recv.at[k, q],
+                (plane - k + planes) % planes * 2 + core,
+                tp,
+            )
+        square = jnp.sum(stream_part * stream_part, 1, keepdims=True)
+        stats_start(1, q, square, square)
+
+    loads[0].wait()
+    for q in (1, 0):
+        projected[pl.ds(q * chunk, chunk), :] = project(q, tp)
+    residual_rows(1)
+    residual_rows(0)
+
+    def spread(k, q):
+        block = tokens.at[row_block(first_row(k, q), chunk), col_block(tp)]
+        landed(block, plane_recv.at[k, q])
+        spread_start(tokens, first_row(k, q), sems(spread_send, k, q), sems(spread_recv, k, q))
+
+    def relay(k, q):
+        spread_relay(tokens, first_row(k, q), sems(spread_send, k, q), sems(spread_recv, k, q))
+
+    def finish(k, q):
+        spread_finish(tokens, first_row(k, q), sems(spread_recv, k, q))
+        block = tokens.at[row_block(first_row(k, q), chunk), :]
+        go(block, block, twin_send.at[k, q], twin_recv.at[k, q], twin, tp)
+
+    def share_scales():
+        for q in range(2):
+            scales[sp, :, pl.ds(q * chunk, chunk)] = lax.rsqrt(
+                stats_total(1, q) / width + epsilon
+            )
+        for i in range(1, n_sp):
+            go(
+                scales.at[sp],
+                scales.at[sp],
+                scale_send.at[i],
+                scale_recv.at[sp],
+                (sp + i) % n_sp,
+                tp,
+            )
+
+    def gather(k):
+        p = (plane + k) % planes
+        for q in range(2):
+            start = (2 * p + 1 - core) * rows + q * chunk
+            landed(tokens.at[row_block(start, chunk), :], twin_recv.at[k, q])
+        for j in range(2):
+            s = 2 * p + (core if j == 0 else 1 - core)
+            if k == 0 and j == 0:
+                pass
+            else:
+                landed(scales.at[s], scale_recv.at[s])
+            here = pl.ds(j * cap, cap)
+            pick = picks[p, here, :]
+            slots[here, :] = jnp.dot(
+                pick, tokens[row_block(s * rows, rows), :], preferred_element_type=jnp.float32
+            ).astype(jnp.bfloat16)
+            scale = jnp.sum(pick.astype(jnp.float32) * scales[s][0:1, :], 1, keepdims=True)
+            since[here, :] = jnp.broadcast_to(scale, (cap, 128))
+
+    def raise_up(k):
+        units = gate.shape[1]
+        tile = min(256, units)
+
+        @pl.loop(0, units // tile)
+        def _(n):
+            at = pl.ds(pl.multiple_of(n * tile, tile), tile)
+            scale = since[0 : 2 * cap, 0:1]
+            g = scale * jnp.dot(slots[...], gate[:, at], preferred_element_type=jnp.float32)
+            u = scale * jnp.dot(slots[...], up[:, at], preferred_element_type=jnp.float32)
+            hidden[:, at] = (g * jax.nn.sigmoid(g) * u).astype(jnp.bfloat16)
+
+    def bring_down(k):
+        @pl.loop(0, width // 256)
+        def _(n):
+            at = pl.ds(pl.multiple_of(n * 256, 256), 256)
+            result = jnp.dot(
+                hidden[...], down[:, at], preferred_element_type=jnp.float32
+            ).astype(jnp.bfloat16)
+            pairs[k, 0:cap, at] = result[0:cap]
+            outbound[k, :, at] = result[cap:]
+
+        go(
+            outbound.at[k],
+            pairs.at[k, pl.ds(cap, cap), :],
+            swap_send.at[k],
+            swap_recv.at[k],
+            twin,
+            tp,
+        )
+
+    low, high = pl.ds(0, chunk), pl.ds(chunk, chunk)
+
+    def combine(k):
+        p = (plane + k) % planes
+        landed(pairs.at[k, pl.ds(cap, cap), :], swap_recv.at[k])
+
+        @pl.loop(0, width // 256)
+        def _(n):
+            at = pl.ds(pl.multiple_of(n * 256, 256), 256)
+            blended[k, :, at] = transposed_dot(blends[p], pairs[k, :, at]).astype(jnp.bfloat16)
+
+        for i, (part_rows, block, peer) in enumerate(
+            (
+                (low, diagonal, across_x),
+                (high, diagonal, across_y),
+                (low, across_x, across_x),
+                (high, across_y, across_y),
+            )
+        ):
+            go(
+                blended.at[k, part_rows, col_block(block)],
+                arrived.at[k, i, low],
+                sum_send.at[k, i],
+                sum_recv.at[k, i],
+                sp,
+                peer,
+            )
+
+    def pass_on(k):
+        for i, (part_rows, peer) in enumerate(((low, across_y), (high, across_x))):
+            landed(arrived.at[k, i, low], sum_recv.at[k, i])
+            arrived[k, 2 + i, high] = (
+                blended[k, part_rows, col_block(peer)].astype(jnp.float32)
+                + arrived[k, i, low].astype(jnp.float32)
+            ).astype(jnp.bfloat16)
+            go(
+                arrived.at[k, 2 + i, high],
+                arrived.at[k, i, high],
+                sum_send.at[k, 4 + i],
+                sum_recv.at[k, 4 + i],
+                sp,
+                peer,
+            )
+
+    def give_back(k):
+        for i, part_rows in enumerate((low, high)):
+            landed(arrived.at[k, 2 + i, low], sum_recv.at[k, 2 + i])
+            landed(arrived.at[k, i, high], sum_recv.at[k, 4 + i])
+            total = (
+                blended[k, part_rows, col_block(tp)].astype(jnp.float32)
+                + arrived[k, 2 + i, low].astype(jnp.float32)
+                + arrived[k, i, high].astype(jnp.float32)
+            )
+            if k == 0:
+                here = pl.ds(i * chunk, chunk)
+                total = total + stream[here, :].astype(jnp.float32)
+                for j in near[1:]:
+                    landed(returned.at[j, part_rows], back_recv.at[j, i])
+                    total = total + returned[j, part_rows].astype(jnp.float32)
+                mixed[here, :] = total.astype(jnp.bfloat16)
+            else:
+                summed[k, part_rows] = total.astype(jnp.bfloat16)
+                go(
+                    summed.at[k, part_rows],
+                    returned.at[k, part_rows],
+                    back_send.at[k, i],
+                    back_recv.at[k, i],
+                    source(k),
+                    tp,
+                )
+
+    near_order = near
+    relay(0, 1)
+    relay(0, 0)
+    share_scales()
+    a, b, c, d = near_order
+    for q in (1, 0):
+        spread(b, q)
+    finish(0, 1)
+    finish(0, 0)
+    for q in (1, 0):
+        relay(b, q)
+        spread(c, q)
+    for load in loads[1:]:
+        load.wait()
+    gather(0)
+    raise_up(0)
+    finish(b, 1)
+    finish(b, 0)
+    relay(c, 1)
+    spread(d, 1)
+    bring_down(0)
+    relay(c, 0)
+    spread(d, 0)
+    gather(b)
+    raise_up(b)
+    finish(c, 1)
+    finish(c, 0)
+    bring_down(b)
+    relay(d, 1)
+    relay(d, 0)
+    combine(b)
+    gather(c)
+    raise_up(c)
+    finish(d, 1)
+    finish(d, 0)
+    bring_down(c)
+    pass_on(b)
+    combine(c)
+    gather(d)
+    raise_up(d)
+    give_back(b)
+    bring_down(d)
+    pass_on(c)
+    combine(d)
+    give_back(c)
+    combine(0)
+    pass_on(d)
+    pass_on(0)
+    give_back(d)
+    give_back(0)
+    for send in sends:
+        send.wait_send()
+
+
+def fused(operands, rows, cols, n_sp, n_tp, cap, width, units, taps):
+    planes = n_sp // 2
+    pad = (taps - 1 + 15) // 16 * 16
+    chunk = rows // 2
+    bf16, f32 = jnp.bfloat16, jnp.float32
+    dma = pltpu.SemaphoreType.DMA
+    vmem = pl.BlockSpec(memory_space=pltpu.VMEM)
+    anywhere = pl.BlockSpec(memory_space=pl.ANY)
+    return pl.pallas_call(
+        functools.partial(fused_kernel, n_sp, n_tp, cap),
+        out_shape=jax.ShapeDtypeStruct((rows, cols), bf16),
+        in_specs=[vmem] * 9 + [anywhere] * 4,
+        out_specs=vmem,
+        scratch_shapes=[
+            pltpu.VMEM((width, cols), bf16),
+            pltpu.VMEM((width, units), bf16),
+            pltpu.VMEM((width, units), bf16),
+            pltpu.VMEM((units, width), bf16),
+            pltpu.VMEM((taps, cols), f32),
+            pltpu.VMEM((pad + rows, cols), f32),
+            pltpu.VMEM((pad + rows, 128), f32),
+            pltpu.VMEM((max(rows, 2 * cap), 128), f32),
+            pltpu.VMEM((rows, cols), f32),
+            pltpu.VMEM((pad, cols), bf16),
+            pltpu.VMEM((pad, 128), f32),
+            pltpu.VMEM((pad, cols), bf16),
+            pltpu.VMEM((pad, 128), f32),
+            pltpu.VMEM((2, 2, n_tp, 8, chunk), f32),
+            pltpu.VMEM((n_sp, 8, rows), f32),
+            pltpu.VMEM((n_sp, 8, rows), f32),
+            pltpu.VMEM((rows, width), bf16),
+            pltpu.VMEM((rows, cols), f32),
+            pltpu.VMEM((rows, cols), bf16),
+            pltpu.VMEM((n_sp * rows, width), bf16),
+            pltpu.VMEM((planes, 2 * cap, rows), bf16),
+            pltpu.VMEM((planes, 2 * cap, rows), bf16),
+            pltpu.VMEM((2 * cap, width), bf16),
+            pltpu.VMEM((2 * cap, units), bf16),
+            pltpu.VMEM((planes, 2 * cap, width), bf16),
+            pltpu.VMEM((planes, cap, width), bf16),
+            pltpu.VMEM((planes, rows, width), bf16),
+            pltpu.VMEM((planes, 4, rows, cols), bf16),
+            pltpu.VMEM((planes, rows, cols), bf16),
+            pltpu.VMEM((planes, rows, cols), bf16),
+            dma((4,)),
+            dma((2,)),
+            dma((2,)),
+            dma((2, 2, n_tp)),
+            dma((2, 2, n_tp)),
+            dma((n_sp,)),
+            dma((n_sp,)),
+            dma((n_sp,)),
+            dma((n_sp,)),
+            dma((2, 4)),
+            dma((2, 4)),
+            dma((planes, 2)),
+            dma((planes, 2)),
+            dma((planes, 2, 4)),
+            dma((planes, 2, 4)),
+            dma((planes, 2)),
+            dma((planes, 2)),
+            dma((planes,)),
+            dma((planes,)),
+            dma((planes, 6)),
+            dma((planes, 6)),
+            dma((planes, 2)),
+            dma((planes, 2)),
+        ],
+        compiler_params=pltpu.CompilerParams(
+            collective_id=0, has_side_effects=True, vmem_limit_bytes=56 << 20
+        ),
+    )(*operands)
+
+
 def per_device(
     residual_in,
     conv_value,
@@ -514,6 +1122,23 @@
     group_rows = n_sp // groups * cap
     taps = conv_kernel.shape[0]
     pad = (taps - 1 + 15) // 16 * 16
+    if n_tp == 4 and n_sp == 8:
+        operands = (
+            residual_in,
+            conv_value,
+            conv_gate,
+            doc_ids.reshape(1, rows),
+            conv_kernel,
+            ln_gain.reshape(cols // 128, 128),
+            norm_gain.reshape(cols // 128, 128),
+            routes.T,
+            route_weight.T,
+            out_weight,
+            gate_w[0],
+            up_w[0],
+            down_w[0],
+        )
+        return fused(operands, rows, cols, n_sp, n_tp, cap, width, units, taps)
     bf16, f32 = jnp.bfloat16, jnp.float32
     dma = pltpu.SemaphoreType.DMA
     vmem = pl.BlockSpec(memory_space=pltpu.VMEM)

time: 131 us -> 114 us (0.87)
  the two profiles are of different devices: /device:TPU:25 before, /device:TPU:0 now
where the time goes in v1:
time: 114 us
  Pallas kernels  112 us (98%)
  local copies, waits for them, and re-layouts  1.67 us (1%)
    pallas_call x1, Pallas kernels, fused(): pl.pallas_call(functools.partial(fused_kernel, n_sp, n_tp, cap), out_shap...  112 us

profile of v1, /device:TPU:0, one launch (start us, length us, event | category | flops | bytes accessed | tf_op | source)
XLA Modules:
  0.0 113.7 jit_solution(8286329215759071855)
XLA Ops:
  0.0 112.1 %shard_map.127 = bf16[256,512]{1,0:T(8,128)(2,1)} custom-call(bf16[256,512]{1,0:T(8,128)(2,1)} %residual.1, bf16[256,512]{1,0:T(8,128)(2,1)} %conv_value.1, bf16[256,512]{1,0:T(8,128)(2,1)} %conv_gate.1, s32[1,256]{1,0:T(1,128)} %bitcast.13, bf16[31,512]{1,0:T(8,128)(2,1)} %conv_kernel.1, bf16[4,128]{1,0:T(4,128)(2,1)} %bitcast.14, bf16[4,128]{1,0:T(4,128)(2,1)} %bitcast.15, ...), custom_call_target="tpu_custom_call" | custom-call | tf_op jit(solution)/shard_map/pallas_call | solution.py:1036
  112.1 1.7 %copy.15 = bf16[256,512]{1,0:T(8,128)(2,1)} copy(bf16[256,512]{1,0:T(8,128)(2,1)} %shard_map.127) | data formatting | bytes 524288

commit v2 on v1

--- a/solution.py
+++ b/solution.py
@@ -489,6 +489,23 @@
     mixed[...] = (stream[...].astype(jnp.float32) + routed).astype(jnp.bfloat16)
     for send in sends:
         send.wait_send()
+
+
+schedule = (
+    "R01", "R00", "H",
+    "S11", "S10",
+    "F01", "F00",
+    "R11", "S21", "R10", "S20", "L",
+    "G0", "U00", "U01",
+    "F11", "F10", "R21", "S31",
+    "D00", "D01", "R20", "S30",
+    "G1", "U10", "U11", "F21", "F20", "D10", "D11",
+    "R31", "R30", "C1",
+    "G2", "U20", "U21", "F31", "F30", "D20", "D21",
+    "P1", "C2",
+    "G3", "U30", "U31", "V1", "D30", "D31",
+    "P2", "C3", "V2", "C0", "P3", "P0", "V3", "V0",
+)
 
 
 def fused_kernel(
@@ -771,15 +788,19 @@
     for p in range(planes):
         slot, weight = mine[p]
         picks[p, 0:cap] = jnp.where(slot == slot_id, 1.0, 0.0).astype(jnp.bfloat16)
-        blends[p, 0:cap] = jnp.where(slot == slot_id, weight, 0.0).astype(jnp.bfloat16)
+        own_blend = jnp.where(slot == slot_id, weight, 0.0)
         slot, weight = rest[p]
         picks[p, cap : 2 * cap] = jnp.where(slot == slot_id, 1.0, 0.0).astype(jnp.bfloat16)
         slot, weight = other[p]
-        blends[p, cap : 2 * cap] = jnp.where(slot == slot_id, weight, 0.0).astype(jnp.bfloat16)
-
-    near = [0]
-    for d in range(1, planes // 2 + 1):
-        near += [d] if 2 * d == planes else [d, planes - d]
+        twin_blend = jnp.where(slot == slot_id, weight, 0.0)
+        blends[p] = jnp.transpose(jnp.concatenate([own_blend, twin_blend], 0)).astype(jnp.bfloat16)
+
+    order = [0] + sorted(range(1, planes), key=lambda k: -min(k, planes - k))
+
+    plane_order = {
+        1: [(order[1], 1)],
+        0: [(order[1], 0)] + [(k, q) for k in order[2:] for q in (1, 0)],
+    }
 
     def source(k):
         return (plane + k) % planes * 2 + core
@@ -802,14 +823,14 @@
         tokens[row_block(first_row(0, q), chunk), col_block(tp)] = (
             stream_part * gain_row(norm_gain)
         ).astype(jnp.bfloat16)
-        block = tokens.at[row_block(first_row(0, q), chunk), col_block(tp)]
         spread_start(tokens, first_row(0, q), sems(spread_send, 0, q), sems(spread_recv, 0, q))
-        for k in near[1:]:
+        for k, part_q in plane_order[q]:
+            block = tokens.at[row_block(first_row(0, part_q), chunk), col_block(tp)]
             go(
                 block,
                 block,
-                plane_send.at[k, q],
-                plane_recv.at[k, q],
+                plane_send.at[k, part_q],
+                plane_recv.at[k, part_q],
                 (plane - k + planes) % planes * 2 + core,
                 tp,
             )
@@ -869,36 +890,31 @@
             scale = jnp.sum(pick.astype(jnp.float32) * scales[s][0:1, :], 1, keepdims=True)
             since[here, :] = jnp.broadcast_to(scale, (cap, 128))
 
-    def raise_up(k):
-        units = gate.shape[1]
-        tile = min(256, units)
-
-        @pl.loop(0, units // tile)
-        def _(n):
-            at = pl.ds(pl.multiple_of(n * tile, tile), tile)
-            scale = since[0 : 2 * cap, 0:1]
-            g = scale * jnp.dot(slots[...], gate[:, at], preferred_element_type=jnp.float32)
-            u = scale * jnp.dot(slots[...], up[:, at], preferred_element_type=jnp.float32)
-            hidden[:, at] = (g * jax.nn.sigmoid(g) * u).astype(jnp.bfloat16)
-
-    def bring_down(k):
-        @pl.loop(0, width // 256)
-        def _(n):
-            at = pl.ds(pl.multiple_of(n * 256, 256), 256)
-            result = jnp.dot(
-                hidden[...], down[:, at], preferred_element_type=jnp.float32
-            ).astype(jnp.bfloat16)
-            pairs[k, 0:cap, at] = result[0:cap]
-            outbound[k, :, at] = result[cap:]
-
-        go(
-            outbound.at[k],
-            pairs.at[k, pl.ds(cap, cap), :],
-            swap_send.at[k],
-            swap_recv.at[k],
-            twin,
-            tp,
-        )
+    def raise_up(k, piece):
+        size = gate.shape[1] // 2
+        at = pl.ds(piece * size, size)
+        scale = jnp.concatenate([since[0 : 2 * cap, :]] * (size // 128), 1)
+        g = scale * jnp.dot(slots[...], gate[:, at], preferred_element_type=jnp.float32)
+        u = scale * jnp.dot(slots[...], up[:, at], preferred_element_type=jnp.float32)
+        hidden[:, at] = (g * jax.nn.sigmoid(g) * u).astype(jnp.bfloat16)
+
+    def bring_down(k, piece):
+        size = width // 2
+        at = pl.ds(piece * size, size)
+        result = jnp.dot(
+            hidden[...], down[:, at], preferred_element_type=jnp.float32
+        ).astype(jnp.bfloat16)
+        pairs[k, 0:cap, at] = result[0:cap]
+        outbound[k, :, at] = result[cap:]
+        if piece == 1:
+            go(
+                outbound.at[k],
+                pairs.at[k, pl.ds(cap, cap), :],
+                swap_send.at[k],
+                swap_recv.at[k],
+                twin,
+                tp,
+            )
 
     low, high = pl.ds(0, chunk), pl.ds(chunk, chunk)
 
@@ -906,10 +922,9 @@
         p = (plane + k) % planes
         landed(pairs.at[k, pl.ds(cap, cap), :], swap_recv.at[k])
 
-        @pl.loop(0, width // 256)
-        def _(n):
-            at = pl.ds(pl.multiple_of(n * 256, 256), 256)
-            blended[k, :, at] = transposed_dot(blends[p], pairs[k, :, at]).astype(jnp.bfloat16)
+        blended[k] = jnp.dot(
+            blends[p], pairs[k], preferred_element_type=jnp.float32
+        ).astype(jnp.bfloat16)
 
         for i, (part_rows, block, peer) in enumerate(
             (
@@ -956,7 +971,7 @@
             if k == 0:
                 here = pl.ds(i * chunk, chunk)
                 total = total + stream[here, :].astype(jnp.float32)
-                for j in near[1:]:
+                for j in order[1:]:
                     landed(returned.at[j, part_rows], back_recv.at[j, i])
                     total = total + returned[j, part_rows].astype(jnp.float32)
                 mixed[here, :] = total.astype(jnp.bfloat16)
@@ -971,56 +986,26 @@
                     tp,
                 )
 
-    near_order = near
-    relay(0, 1)
-    relay(0, 0)
-    share_scales()
-    a, b, c, d = near_order
-    for q in (1, 0):
-        spread(b, q)
-    finish(0, 1)
-    finish(0, 0)
-    for q in (1, 0):
-        relay(b, q)
-        spread(c, q)
-    for load in loads[1:]:
-        load.wait()
-    gather(0)
-    raise_up(0)
-    finish(b, 1)
-    finish(b, 0)
-    relay(c, 1)
-    spread(d, 1)
-    bring_down(0)
-    relay(c, 0)
-    spread(d, 0)
-    gather(b)
-    raise_up(b)
-    finish(c, 1)
-    finish(c, 0)
-    bring_down(b)
-    relay(d, 1)
-    relay(d, 0)
-    combine(b)
-    gather(c)
-    raise_up(c)
-    finish(d, 1)
-    finish(d, 0)
-    bring_down(c)
-    pass_on(b)
-    combine(c)
-    gather(d)
-    raise_up(d)
-    give_back(b)
-    bring_down(d)
-    pass_on(c)
-    combine(d)
-    give_back(c)
-    combine(0)
-    pass_on(d)
-    pass_on(0)
-    give_back(d)
-    give_back(0)
+    def weights_ready():
+        for load in loads[1:]:
+            load.wait()
+
+    steps = {
+        "R": relay,
+        "S": spread,
+        "F": finish,
+        "G": gather,
+        "U": raise_up,
+        "D": bring_down,
+        "C": combine,
+        "P": pass_on,
+        "V": give_back,
+        "H": share_scales,
+        "L": weights_ready,
+    }
+    for word in schedule:
+        indices = [int(digit) for digit in word[1:]]
+        steps[word[0]](*[order[i] for i in indices[:1]], *indices[1:])
     for send in sends:
         send.wait_send()
 
@@ -1060,7 +1045,7 @@
             pltpu.VMEM((rows, cols), bf16),
             pltpu.VMEM((n_sp * rows, width), bf16),
             pltpu.VMEM((planes, 2 * cap, rows), bf16),
-            pltpu.VMEM((planes, 2 * cap, rows), bf16),
+            pltpu.VMEM((planes, rows, 2 * cap), bf16),
             pltpu.VMEM((2 * cap, width), bf16),
             pltpu.VMEM((2 * cap, units), bf16),
             pltpu.VMEM((planes, 2 * cap, width), bf16),

time: 114 us -> 107 us (0.939); the launches traced: 114 us -> 105 us
  Pallas kernels: 112 us -> 103 us
    pallas_call x1, Pallas kernels: 112 us -> 103 us  [fused(): pl.pallas_call(functools.partial(fused_kernel, n_sp, n_tp, cap), out_shap...]
where the time goes in v2:
time: 107 us; the launch traced here: 105 us
  Pallas kernels  103 us (96%)
  local copies, waits for them, and re-layouts  1.67 us (2%)
    pallas_call x1, Pallas kernels, fused(): pl.pallas_call(functools.partial(fused_kernel, n_sp, n_tp, cap), out_shap...  103 us

profile of v2, /device:TPU:0, one launch (start us, length us, event | category | flops | bytes accessed | tf_op | source)
XLA Modules:
  0.0 104.7 jit_solution(14035911597257210191)
XLA Ops:
  0.0 103.0 %shard_map.127 = bf16[256,512]{1,0:T(8,128)(2,1)} custom-call(bf16[256,512]{1,0:T(8,128)(2,1)} %residual.1, bf16[256,512]{1,0:T(8,128)(2,1)} %conv_value.1, bf16[256,512]{1,0:T(8,128)(2,1)} %conv_gate.1, s32[1,256]{1,0:T(1,128)} %bitcast.13, bf16[31,512]{1,0:T(8,128)(2,1)} %conv_kernel.1, bf16[4,128]{1,0:T(4,128)(2,1)} %bitcast.14, bf16[4,128]{1,0:T(4,128)(2,1)} %bitcast.15, ...), custom_call_target="tpu_custom_call" | custom-call | tf_op jit(solution)/shard_map/pallas_call | solution.py:1021
  103.0 1.7 %copy.15 = bf16[256,512]{1,0:T(8,128)(2,1)} copy(bf16[256,512]{1,0:T(8,128)(2,1)} %shard_map.127) | data formatting | bytes 524288

commit v3 on v2

--- a/solution.py
+++ b/solution.py
@@ -504,7 +504,7 @@
     "G2", "U20", "U21", "F31", "F30", "D20", "D21",
     "P1", "C2",
     "G3", "U30", "U31", "V1", "D30", "D31",
-    "P2", "C3", "V2", "C0", "P3", "P0", "V3", "V0",
+    "P2", "C3", "V2", "P3", "C0", "V3", "P0", "V0",
 )
 
 

time: 107 us -> 101 us (0.944); the launches traced: 105 us -> 101 us
  Pallas kernels: 103 us -> 99.2 us
    pallas_call x1, Pallas kernels: 103 us -> 99.2 us  [fused(): pl.pallas_call(functools.partial(fused_kernel, n_sp, n_tp, cap), out_shap...]
where the time goes in v3:
time: 101 us
  Pallas kernels  99.2 us (98%)
  local copies, waits for them, and re-layouts  1.67 us (2%)
    pallas_call x1, Pallas kernels, fused(): pl.pallas_call(functools.partial(fused_kernel, n_sp, n_tp, cap), out_shap...  99.2 us

profile of v3, /device:TPU:0, one launch (start us, length us, event | category | flops | bytes accessed | tf_op | source)
XLA Modules:
  0.0 100.9 jit_solution(3551450946008238061)
XLA Ops:
  0.0 99.2 %shard_map.127 = bf16[256,512]{1,0:T(8,128)(2,1)} custom-call(bf16[256,512]{1,0:T(8,128)(2,1)} %residual.1, bf16[256,512]{1,0:T(8,128)(2,1)} %conv_value.1, bf16[256,512]{1,0:T(8,128)(2,1)} %conv_gate.1, s32[1,256]{1,0:T(1,128)} %bitcast.13, bf16[31,512]{1,0:T(8,128)(2,1)} %conv_kernel.1, bf16[4,128]{1,0:T(4,128)(2,1)} %bitcast.14, bf16[4,128]{1,0:T(4,128)(2,1)} %bitcast.15, ...), custom_call_target="tpu_custom_call" | custom-call | tf_op jit(solution)/shard_map/pallas_call | solution.py:1021
  99.2 1.7 %copy.15 = bf16[256,512]{1,0:T(8,128)(2,1)} copy(bf16[256,512]{1,0:T(8,128)(2,1)} %shard_map.127) | data formatting | bytes 524288

commit v4 on v3

--- a/solution.py
+++ b/solution.py
@@ -495,14 +495,14 @@
     "R01", "R00", "H",
     "S11", "S10",
     "F01", "F00",
-    "R11", "S21", "R10", "S20", "L",
+    "R11", "S21", "R10", "S20", "B", "L",
     "G0", "U00", "U01",
     "F11", "F10", "R21", "S31",
-    "D00", "D01", "R20", "S30",
+    "D00", "D01", "R20",
     "G1", "U10", "U11", "F21", "F20", "D10", "D11",
-    "R31", "R30", "C1",
-    "G2", "U20", "U21", "F31", "F30", "D20", "D21",
-    "P1", "C2",
+    "R31", "C1",
+    "G2", "U20", "U21", "F31", "P1", "D20", "D21",
+    "F30", "C2",
     "G3", "U30", "U31", "V1", "D30", "D31",
     "P2", "C3", "V2", "P3", "C0", "V3", "P0", "V0",
 )
@@ -591,7 +591,7 @@
     core = sp % 2
     twin = plane * 2 + 1 - core
     chunk = rows // 2
-    half = chunk // 2
+    strip = rows // 4
     across_x = tp + 1 - 2 * (tp % 2)
     across_y = (tp + 2) % n_tp
     diagonal = (across_x + 2) % n_tp
@@ -629,42 +629,46 @@
     def row_block(start, size):
         return pl.ds(pl.multiple_of(start, size), size)
 
-    def spread_start(ref, start, ss, rs):
-        block = ref.at[row_block(start, chunk), col_block(tp)]
+    def spread_start(ref, start, size, ss, rs):
+        block = ref.at[row_block(start, size), col_block(tp)]
         go(block, block, ss(1), rs(1), sp, across_x)
         go(block, block, ss(2), rs(2), sp, across_y)
 
-    def spread_relay(ref, start, ss, rs):
-        landed(ref.at[row_block(start, chunk), col_block(across_x)], rs(1))
+    def spread_relay(ref, start, size, ss, rs):
+        half = size // 2
+        landed(ref.at[row_block(start, size), col_block(across_x)], rs(1))
         block = ref.at[row_block(start, half), col_block(across_x)]
         go(block, block, ss(3), rs(3), sp, across_y)
-        landed(ref.at[row_block(start, chunk), col_block(across_y)], rs(2))
+        landed(ref.at[row_block(start, size), col_block(across_y)], rs(2))
         block = ref.at[row_block(start + half, half), col_block(across_y)]
         go(block, block, ss(0), rs(0), sp, across_x)
 
-    def spread_finish(ref, start, rs):
+    def spread_finish(ref, start, size, rs):
+        half = size // 2
         landed(ref.at[row_block(start, half), col_block(diagonal)], rs(3))
         landed(ref.at[row_block(start + half, half), col_block(diagonal)], rs(0))
 
-    def stats_start(i, q, first, second):
-        lane = lax.broadcasted_iota(jnp.int32, (chunk, 128), 1)
+    def stats_start(i, first, second):
+        lane = lax.broadcasted_iota(jnp.int32, (first.shape[0], 128), 1)
         both = jnp.where(lane == 0, first, jnp.where(lane == 1, second, 0.0))
-        stats[i, q, 0] = jnp.transpose(both)[0:8]
+        if first.shape[0] < 128:
+            both = jnp.concatenate([both, jnp.zeros((128 - first.shape[0], 128), jnp.float32)], 0)
+        stats[i, 0] = jnp.transpose(both)[0:8]
         for j in range(1, n_tp):
             go(
-                stats.at[i, q, 0],
-                stats.at[i, q, j],
-                stat_send.at[i, q, j],
-                stat_recv.at[i, q, j],
+                stats.at[i, 0],
+                stats.at[i, j],
+                stat_send.at[i, j],
+                stat_recv.at[i, j],
                 sp,
                 (tp + j) % n_tp,
             )
 
-    def stats_total(i, q):
-        total = stats[i, q, 0]
+    def stats_total(i):
+        total = stats[i, 0]
         for j in range(1, n_tp):
-            landed(stats.at[i, q, j], stat_recv.at[i, q, j])
-            total = total + stats[i, q, j]
+            landed(stats.at[i, j], stat_recv.at[i, j])
+            total = total + stats[i, j]
         return total
 
     def gain_row(ref):
@@ -691,7 +695,7 @@
     for i in range(1, n_sp):
         go(plans.at[sp], plans.at[sp], plan_send.at[i], plan_recv.at[sp], (sp + i) % n_sp, tp)
 
-    part = min(64, chunk)
+    part = strip
 
     def convolve(r):
         here = pl.ds(r * part, part)
@@ -701,25 +705,21 @@
             count = count + jnp.where(
                 doc_extended[pl.ds(pad + r * part - back, part), :] == own, 1.0, 0.0
             )
-        since[here, :] = count
-
-        @pl.loop(0, cols // 128)
-        def _(c):
-            at = pl.ds(pl.multiple_of(c * 128, 128), 128)
-            reach = since[here, :]
-            total = jnp.zeros((part, 128), jnp.float32)
-            for tap in range(lookback + 1):
-                value = extended[pl.ds(pad - lookback + r * part + tap, part), at]
-                total = total + jnp.where(
-                    reach >= lookback - tap, value * taps[tap : tap + 1, at], 0.0
-                )
-            conv[here, at] = total
-
-    def channel_stats(q):
-        conv_out = conv[pl.ds(q * chunk, chunk), :]
+        blocks = [pl.ds(c * 128, 128) for c in range(cols // 128)]
+        totals = [jnp.zeros((part, 128), jnp.float32) for _ in blocks]
+        for tap in range(lookback + 1):
+            near = count >= lookback - tap
+            rows_of_tap = pl.ds(pad - lookback + r * part + tap, part)
+            for c, at in enumerate(blocks):
+                value = extended[rows_of_tap, at] * taps[tap : tap + 1, at]
+                totals[c] = totals[c] + jnp.where(near, value, 0.0)
+        for c, at in enumerate(blocks):
+            conv[here, at] = totals[c]
+
+    def channel_stats(r):
+        conv_out = conv[pl.ds(r * strip, strip), :]
         stats_start(
-            0,
-            q,
+            r,
             jnp.sum(conv_out, 1, keepdims=True),
             jnp.sum(conv_out * conv_out, 1, keepdims=True),
         )
@@ -727,28 +727,26 @@
     def sems(ref, *index):
         return lambda i: ref.at[(*index, i)]
 
-    def activate(q):
-        here = pl.ds(q * chunk, chunk)
-        back = jnp.transpose(jnp.concatenate([stats_total(0, q)] * 16, 0))
+    def activate(r):
+        here = pl.ds(r * strip, strip)
+        back = jnp.transpose(jnp.concatenate([stats_total(r)] * 16, 0))[0:strip]
         mean = back[:, 0:1] / width
         scale = lax.rsqrt(back[:, 1:2] / width - mean * mean + epsilon)
         v = (conv[here, :] - mean) * scale * gain_row(ln_gain)
         activated[here, col_block(tp)] = (v * jax.nn.sigmoid(v)).astype(jnp.bfloat16)
-        spread_start(activated, q * chunk, sems(act_send, q), sems(act_recv, q))
-
-    def project(q, t):
+        spread_start(activated, r * strip, strip, sems(act_send, r), sems(act_recv, r))
+
+    def project(r, t):
         return jnp.dot(
-            activated[pl.ds(q * chunk, chunk), col_block(t)],
+            activated[pl.ds(r * strip, strip), col_block(t)],
             proj[col_block(t), :],
             preferred_element_type=jnp.float32,
         )
 
-    parts = chunk // part
-    for r in range(parts, 2 * parts):
+    for r in (3, 2, 1):
         convolve(r)
-    channel_stats(1)
-    for r in range(1, parts):
-        convolve(r)
+        channel_stats(r)
+    activate(3)
     landed(halo, halo_recv.at[0])
     landed(halo_docs, halo_recv.at[1])
     inside = sp > 0
@@ -756,8 +754,8 @@
     doc_extended[pl.ds(0, pad), :] = jnp.where(inside, halo_docs[...], -1.0)
     convolve(0)
     channel_stats(0)
-    activate(1)
-    activate(0)
+    for r in (2, 1, 0):
+        activate(r)
 
     for i in range(1, n_sp):
         e = (sp + i) % n_sp
@@ -799,7 +797,7 @@
 
     plane_order = {
         1: [(order[1], 1)],
-        0: [(order[1], 0)] + [(k, q) for k in order[2:] for q in (1, 0)],
+        0: [(order[1], 0)] + [(k, q) for k in order[2:] for q in (1, 0) if (k, q) != (order[-1], 0)],
     }
 
     def source(k):
@@ -808,22 +806,28 @@
     def first_row(k, q):
         return source(k) * rows + q * chunk
 
-    def residual_rows(q):
-        here = pl.ds(q * chunk, chunk)
-        spread_relay(activated, q * chunk, sems(act_send, q), sems(act_recv, q))
-        projected[here, :] += project(q, across_x) + project(q, across_y)
-        spread_finish(activated, q * chunk, sems(act_recv, q))
-        total = projected[here, :] + project(q, diagonal)
+    def relay_strip(r):
+        spread_relay(activated, r * strip, strip, sems(act_send, r), sems(act_recv, r))
+        here = pl.ds(r * strip, strip)
+        projected[here, :] += project(r, across_x) + project(r, across_y)
+
+    def settle(r):
+        here = pl.ds(r * strip, strip)
+        spread_finish(activated, r * strip, strip, sems(act_recv, r))
+        total = projected[here, :] + project(r, diagonal)
         stream_rows = (
             residual[here, :].astype(jnp.float32)
             + total.astype(jnp.bfloat16).astype(jnp.float32)
         ).astype(jnp.bfloat16)
         stream[here, :] = stream_rows
-        stream_part = stream_rows.astype(jnp.float32)
-        tokens[row_block(first_row(0, q), chunk), col_block(tp)] = (
-            stream_part * gain_row(norm_gain)
+        tokens[row_block(sp * rows + r * strip, strip), col_block(tp)] = (
+            stream_rows.astype(jnp.float32) * gain_row(norm_gain)
         ).astype(jnp.bfloat16)
-        spread_start(tokens, first_row(0, q), sems(spread_send, 0, q), sems(spread_recv, 0, q))
+
+    def send_tokens(q):
+        spread_start(
+            tokens, first_row(0, q), chunk, sems(spread_send, 0, q), sems(spread_recv, 0, q)
+        )
         for k, part_q in plane_order[q]:
             block = tokens.at[row_block(first_row(0, part_q), chunk), col_block(tp)]
             go(
@@ -834,32 +838,56 @@
                 (plane - k + planes) % planes * 2 + core,
                 tp,
             )
+        stream_part = stream[pl.ds(q * chunk, chunk), :].astype(jnp.float32)
         square = jnp.sum(stream_part * stream_part, 1, keepdims=True)
-        stats_start(1, q, square, square)
+        stats_start(4 + q, square, square)
 
     loads[0].wait()
-    for q in (1, 0):
-        projected[pl.ds(q * chunk, chunk), :] = project(q, tp)
-    residual_rows(1)
-    residual_rows(0)
+    for r in (3, 2, 1, 0):
+        projected[pl.ds(r * strip, strip), :] = project(r, tp)
+    relay_strip(3)
+    relay_strip(2)
+    settle(3)
+    relay_strip(1)
+    settle(2)
+    send_tokens(1)
+    relay_strip(0)
+    settle(1)
+    settle(0)
+    send_tokens(0)
 
     def spread(k, q):
         block = tokens.at[row_block(first_row(k, q), chunk), col_block(tp)]
         landed(block, plane_recv.at[k, q])
-        spread_start(tokens, first_row(k, q), sems(spread_send, k, q), sems(spread_recv, k, q))
+        spread_start(tokens, first_row(k, q), chunk, sems(spread_send, k, q), sems(spread_recv, k, q))
 
     def relay(k, q):
-        spread_relay(tokens, first_row(k, q), sems(spread_send, k, q), sems(spread_recv, k, q))
+        spread_relay(tokens, first_row(k, q), chunk, sems(spread_send, k, q), sems(spread_recv, k, q))
+
+    def send_wide():
+        k = order[-1]
+        block = tokens.at[row_block(first_row(0, 0), chunk), :]
+        go(
+            block,
+            block,
+            plane_send.at[k, 0],
+            plane_recv.at[k, 0],
+            (plane - k + planes) % planes * 2 + core,
+            tp,
+        )
 
     def finish(k, q):
-        spread_finish(tokens, first_row(k, q), sems(spread_recv, k, q))
         block = tokens.at[row_block(first_row(k, q), chunk), :]
+        if (k, q) == (order[-1], 0):
+            landed(block, plane_recv.at[k, q])
+        else:
+            spread_finish(tokens, first_row(k, q), chunk, sems(spread_recv, k, q))
         go(block, block, twin_send.at[k, q], twin_recv.at[k, q], twin, tp)
 
     def share_scales():
         for q in range(2):
             scales[sp, :, pl.ds(q * chunk, chunk)] = lax.rsqrt(
-                stats_total(1, q) / width + epsilon
+                stats_total(4 + q) / width + epsilon
             )
         for i in range(1, n_sp):
             go(
@@ -1000,6 +1028,7 @@
         "C": combine,
         "P": pass_on,
         "V": give_back,
+        "B": send_wide,
         "H": share_scales,
         "L": weights_ready,
     }
@@ -1037,7 +1066,7 @@
             pltpu.VMEM((pad, 128), f32),
             pltpu.VMEM((pad, cols), bf16),
             pltpu.VMEM((pad, 128), f32),
-            pltpu.VMEM((2, 2, n_tp, 8, chunk), f32),
+            pltpu.VMEM((6, n_tp, 8, 128), f32),
             pltpu.VMEM((n_sp, 8, rows), f32),
             pltpu.VMEM((n_sp, 8, rows), f32),
             pltpu.VMEM((rows, width), bf16),
@@ -1057,14 +1086,14 @@
             dma((4,)),
             dma((2,)),
             dma((2,)),
-            dma((2, 2, n_tp)),
-            dma((2, 2, n_tp)),
+            dma((6, n_tp)),
+            dma((6, n_tp)),
             dma((n_sp,)),
             dma((n_sp,)),
             dma((n_sp,)),
             dma((n_sp,)),
-            dma((2, 4)),
-            dma((2, 4)),
+            dma((4, 4)),
+            dma((4, 4)),
             dma((planes, 2)),
             dma((planes, 2)),
             dma((planes, 2, 4)),

time: 101 us -> 98.8 us (0.978); the launches traced: 101 us -> 97.6 us
  Pallas kernels: 99.2 us -> 95.9 us
    pallas_call x1, Pallas kernels: 99.2 us -> 95.9 us  [fused(): pl.pallas_call(functools.partial(fused_kernel, n_sp, n_tp, cap), out_shap...]
where the time goes in v4:
time: 98.8 us; the launch traced here: 97.6 us
  Pallas kernels  95.9 us (97%)
  local copies, waits for them, and re-layouts  1.67 us (2%)
    pallas_call x1, Pallas kernels, fused(): pl.pallas_call(functools.partial(fused_kernel, n_sp, n_tp, cap), out_shap...  95.9 us

profile of v4, /device:TPU:0, one launch (start us, length us, event | category | flops | bytes accessed | tf_op | source)
XLA Modules:
  0.0 97.6 jit_solution(16368322555128424827)
XLA Ops:
  0.0 95.9 %shard_map.127 = bf16[256,512]{1,0:T(8,128)(2,1)} custom-call(bf16[256,512]{1,0:T(8,128)(2,1)} %residual.1, bf16[256,512]{1,0:T(8,128)(2,1)} %conv_value.1, bf16[256,512]{1,0:T(8,128)(2,1)} %conv_gate.1, s32[1,256]{1,0:T(1,128)} %bitcast.13, bf16[31,512]{1,0:T(8,128)(2,1)} %conv_kernel.1, bf16[4,128]{1,0:T(4,128)(2,1)} %bitcast.14, bf16[4,128]{1,0:T(4,128)(2,1)} %bitcast.15, ...), custom_call_target="tpu_custom_call" | custom-call | tf_op jit(solution)/shard_map/pallas_call | solution.py:1050
  96.0 1.7 %copy.15 = bf16[256,512]{1,0:T(8,128)(2,1)} copy(bf16[256,512]{1,0:T(8,128)(2,1)} %shard_map.127) | data formatting | bytes 524288

commit v5 on v4

--- a/solution.py
+++ b/solution.py
@@ -492,19 +492,7 @@
 
 
 schedule = (
-    "R01", "R00", "H",
-    "S11", "S10",
-    "F01", "F00",
-    "R11", "S21", "R10", "S20", "B", "L",
-    "G0", "U00", "U01",
-    "F11", "F10", "R21", "S31",
-    "D00", "D01", "R20",
-    "G1", "U10", "U11", "F21", "F20", "D10", "D11",
-    "R31", "C1",
-    "G2", "U20", "U21", "F31", "P1", "D20", "D21",
-    "F30", "C2",
-    "G3", "U30", "U31", "V1", "D30", "D31",
-    "P2", "C3", "V2", "P3", "C0", "V3", "P0", "V0",
+    "R01", "H", "S11", "R00", "R11", "S10", "F00", "F01", "L", "S21", "G0", "U00", "R10", "U01", "F11", "D00", "S20", "F10", "S31", "R21", "D01", "B", "G1", "U11", "R20", "U10", "D10", "D11", "R31", "F21", "C1", "F20", "G2", "U20", "F31", "U21", "P1", "D20", "D21", "C2", "F30", "V1", "G3", "U30", "U31", "P2", "D30", "D31", "C3", "V2", "P3", "C0", "V3", "P0", "V0",
 )
 
 

time: 98.8 us -> 98.1 us (level); the launches traced: 97.6 us -> 97.9 us
  no operation moved by 1% of the time
where the time goes in v5:
time: 98.1 us; the launch traced here: 97.9 us
  Pallas kernels  96.3 us (98%)
  local copies, waits for them, and re-layouts  1.67 us (2%)
    pallas_call x1, Pallas kernels, fused(): pl.pallas_call(functools.partial(fused_kernel, n_sp, n_tp, cap), out_shap...  96.3 us

profile of v5, /device:TPU:0, one launch (start us, length us, event | category | flops | bytes accessed | tf_op | source)
XLA Modules:
  0.0 97.9 jit_solution(7218304131592030246)
XLA Ops:
  0.0 96.3 %shard_map.127 = bf16[256,512]{1,0:T(8,128)(2,1)} custom-call(bf16[256,512]{1,0:T(8,128)(2,1)} %residual.1, bf16[256,512]{1,0:T(8,128)(2,1)} %conv_value.1, bf16[256,512]{1,0:T(8,128)(2,1)} %conv_gate.1, s32[1,256]{1,0:T(1,128)} %bitcast.13, bf16[31,512]{1,0:T(8,128)(2,1)} %conv_kernel.1, bf16[4,128]{1,0:T(4,128)(2,1)} %bitcast.14, bf16[4,128]{1,0:T(4,128)(2,1)} %bitcast.15, ...), custom_call_target="tpu_custom_call" | custom-call | tf_op jit(solution)/shard_map/pallas_call | solution.py:1038
  96.3 1.7 %copy.15 = bf16[256,512]{1,0:T(8,128)(2,1)} copy(bf16[256,512]{1,0:T(8,128)(2,1)} %shard_map.127) | data formatting | bytes 524288
